TPU v7x, 256 devices: a whole 4x4x8 slice. The times are simulated.
256 devices in a mesh: sp: 32 (over z, x), tp: 8 (over y, core).
Axes of the slice: x: 4, y: 4, z: 8, core: 2. Of those that a mesh axis runs over, the one named last changes fastest.
Arguments:
- latents: bfloat16 [16384, 2048], P(('sp', 'tp')), may hold values from -6 to 6
- context: bfloat16 [512, 2048], P('sp'), may hold values from -6 to 6
- cond: float32 [2048], P('sp'), may hold values from -6 to 6
- ctx_cond: float32 [2048], P('sp'), may hold values from -6 to 6
- mod_weight: float32 [2048, 6144], P('sp', 'tp'), may hold values from -0.125 to 0.125
- query_weight: bfloat16 [2048, 2048], P(None, 'tp'), may hold values from -1 to 1, as said below
- key_matrix: bfloat16 [2048, 1024], P(None, 'tp'), may hold values from -1 to 1, as said below
- value_matrix: bfloat16 [2048, 1024], P(None, 'tp'), may hold values from -0.125 to 0.125
- out_weight: bfloat16 [2048, 2048], P('tp'), may hold values from -0.125 to 0.125
- query_gain: float32 [128], replicated, may hold values from 0.7 to 7
- key_gain: float32 [128], replicated, may hold values from 0.7 to 7
Outputs:
- updated: bfloat16 [16384, 2048], P(('sp', 'tp'))
Inputs may be any that keep to these rules, and one draw needn't show every extreme that they name: `query_weight`: entries of order 2048 to the power -1/2. `key_matrix`: entries of order 2048 to the power -1/2.
All inputs are finite; a program needn't handle non-finite values.
Results may differ from a plain program's by a relative error of at most 0.0085.
The roundings to bfloat16 on the way count: a program that leaves them out, or rounds other values in their place, can miss the bound.
Values may be sent and summed in bfloat16 or wider, within the bound.
No kernel may reach another device: no remote copies, remote signals or barrier semaphores. Data moves between devices by JAX's collectives and lax.ppermute only.
A program may use at most 128 MiB of HBM per device.

v0:
```python
import math
import jax
import jax.numpy as jnp
from jax import lax
from jax.sharding import Mesh
from jax.sharding import PartitionSpec as P

GRID_W = 64
SP = ("sp_0", "sp_1")
SP_TP = ("sp_0", "sp_1", "tp")
NORM_EPS = 1e-06
ROPE_BASE = 10000.0


def over_axes(value, axes):
    for axis in axes:
        value = lax.psum(value, axis)
    return value


def side_by_side(arrays, axis, dim, along):
    both = jnp.concatenate(arrays, axis=along)
    filled, at, done = (lax.all_gather(both, axis, axis=dim, tiled=True), 0, [])
    for a in arrays:
        done.append(lax.slice_in_dim(filled, at, at + a.shape[along], axis=along))
        at += a.shape[along]
    return tuple(done)


def normalize(latent_value_rows):
    return latent_value_rows * lax.rsqrt(
        jnp.mean(latent_value_rows * latent_value_rows, axis=-1, keepdims=True) + NORM_EPS
    )


def rotate(latent_value_rows, positions):
    quarter = latent_value_rows.shape[-1] // 2
    inv_freq = ROPE_BASE ** (-jnp.arange(quarter, dtype=jnp.float32) / quarter)
    angles = positions.astype(jnp.float32)[:, None] * inv_freq[None, :]
    cos_table = jnp.cos(angles)[:, None, :]
    sin_table = jnp.sin(angles)[:, None, :]
    first, second = (latent_value_rows[..., :quarter], latent_value_rows[..., quarter:])
    return jnp.concatenate(
        [first * cos_table - second * sin_table, second * cos_table + first * sin_table], axis=-1
    )


def axial(latent_value_rows, positions):
    half_dim = latent_value_rows.shape[-1] // 2
    return jnp.concatenate(
        [
            rotate(latent_value_rows[..., :half_dim], positions // GRID_W),
            rotate(latent_value_rows[..., half_dim:], positions % GRID_W),
        ],
        axis=-1,
    )


def modulate(latent_value_rows, mod_row):
    model_width = latent_value_rows.shape[-1]
    shift_vec = mod_row[:model_width]
    scale_vec = mod_row[model_width : 2 * model_width]
    return (
        normalize(latent_value_rows.astype(jnp.float32)) * (1.0 + scale_vec) + shift_vec
    ).astype(jnp.bfloat16)


def body(
    latents,
    context,
    cond,
    ctx_cond,
    mod_weight,
    query_weight,
    key_matrix,
    value_matrix,
    out_weight,
    query_gain,
    key_gain,
):
    model_width = latents.shape[1]
    head_dim = query_gain.shape[0]
    sp_count = lax.axis_size(SP)
    partials = jnp.dot(
        jax.nn.silu(jnp.stack([cond, ctx_cond])), mod_weight, precision=lax.Precision.HIGHEST
    )
    summed = over_axes(partials, SP)
    modulation = lax.all_gather(summed, "tp", axis=1, tiled=True)
    gate_vec = modulation[0, 2 * model_width :]
    normalised_rows = modulate(latents, modulation[0])
    prefix_normalised = modulate(context, modulation[1])
    query_cols = query_weight.shape[1]
    key_cols = key_matrix.shape[1]
    piece = lax.all_gather(normalised_rows, "tp", axis=0, tiled=True)
    projected = jnp.concatenate(
        [
            jnp.dot(piece, query_weight, preferred_element_type=jnp.float32),
            jnp.dot(piece, key_matrix, preferred_element_type=jnp.float32),
            jnp.dot(piece, value_matrix, preferred_element_type=jnp.float32),
        ],
        axis=1,
    )
    row_count = projected.shape[0]
    positions = lax.axis_index(SP) * row_count + jnp.arange(row_count, dtype=jnp.int32)
    query_heads = projected[:, :query_cols].reshape(row_count, -1, head_dim)
    query_heads = axial(normalize(query_heads) * query_gain, positions).astype(jnp.bfloat16)
    key_heads = projected[:, query_cols : query_cols + key_cols].reshape(row_count, -1, head_dim)
    key_heads = axial(normalize(key_heads) * key_gain, positions).astype(jnp.bfloat16)
    value_heads = (
        projected[:, query_cols + key_cols :].reshape(row_count, -1, head_dim).astype(jnp.bfloat16)
    )
    key_part = jnp.dot(prefix_normalised, key_matrix, preferred_element_type=jnp.float32).reshape(
        prefix_normalised.shape[0], -1, head_dim
    )
    value_part = jnp.dot(
        prefix_normalised, value_matrix, preferred_element_type=jnp.float32
    ).reshape(prefix_normalised.shape[0], -1, head_dim)
    local_keys = (normalize(key_part) * key_gain).astype(jnp.bfloat16)
    local_values = value_part.astype(jnp.bfloat16)
    prefix_keys, prefix_values = side_by_side((local_keys, local_values), SP, 0, 1)
    kv_local = key_heads.shape[1]
    group_size = query_heads.shape[1] // kv_local
    grouped = query_heads.reshape(row_count, kv_local, group_size, head_dim).transpose(1, 2, 0, 3)
    grouped = grouped.reshape(kv_local, group_size * row_count, head_dim)
    inv_root = head_dim ** (-0.5)
    lift = math.log(sp_count * row_count / (2.0 * prefix_keys.shape[0]))
    ctx_scores = (
        jnp.einsum("hqd,khd->hqk", grouped, prefix_keys, preferred_element_type=jnp.float32)
        * inv_root
        + lift
    )
    top_init = jnp.max(ctx_scores, axis=-1)
    ctx_weights = jnp.exp(ctx_scores - top_init[..., None])
    initial = (
        top_init,
        jnp.sum(ctx_weights, axis=-1),
        jnp.einsum(
            "hqk,khd->hqd",
            ctx_weights.astype(jnp.bfloat16),
            prefix_values,
            preferred_element_type=jnp.float32,
        ),
    )

    def update(state_now, key_block, value_block):
        top_old, total_old, acc_old = state_now
        scores = (
            jnp.einsum("hqd,khd->hqk", grouped, key_block, preferred_element_type=jnp.float32)
            * inv_root
        )
        top_new = jnp.maximum(top_old, jnp.max(scores, axis=-1))
        factor = jnp.exp(top_old - top_new)
        weights_now = jnp.exp(scores - top_new[..., None])
        acc_new = acc_old * factor[..., None] + jnp.einsum(
            "hqk,khd->hqd",
            weights_now.astype(jnp.bfloat16),
            value_block,
            preferred_element_type=jnp.float32,
        )
        return (top_new, total_old * factor + jnp.sum(weights_now, axis=-1), acc_new)

    key_piece, value_piece = side_by_side((key_heads, value_heads), SP, 0, 1)
    key_count = key_piece.shape[0]
    rows_per_block = math.gcd(key_count, 2048)
    block_count = key_count // rows_per_block
    key_blocks = key_piece.reshape(block_count, rows_per_block, kv_local, head_dim)
    value_blocks = value_piece.reshape(block_count, rows_per_block, kv_local, head_dim)

    def one_step(state_in, blocks_in):
        return (update(state_in, blocks_in[0], blocks_in[1]), None)

    state_out, _ = lax.scan(one_step, initial, (key_blocks, value_blocks))
    top_fin, total_fin, acc_fin = state_out
    attended = (acc_fin / total_fin[..., None]).astype(jnp.bfloat16)
    attended = (
        attended.reshape(kv_local, group_size, row_count, head_dim)
        .transpose(2, 0, 1, 3)
        .reshape(row_count, -1)
    )
    exchanged = lax.all_to_all(attended, "tp", split_axis=0, concat_axis=1, tiled=True)
    mixed_rows = jnp.dot(
        exchanged,
        lax.all_gather(out_weight, "tp", axis=0, tiled=True),
        preferred_element_type=jnp.float32,
    )
    return (latents.astype(jnp.float32) + gate_vec * normalize(mixed_rows)).astype(jnp.bfloat16)


def solution(mesh):
    torus = Mesh(mesh.devices.reshape(8, 4, mesh.shape["tp"]), ("sp_0", "sp_1", "tp"))
    placed = (
        P(SP_TP, None),
        P(SP, None),
        P(SP),
        P(SP),
        P(SP, "tp"),
        P(None, "tp"),
        P(None, "tp"),
        P(None, "tp"),
        P("tp", None),
        P(),
        P(),
    )
    return jax.shard_map(
        body, mesh=torus, in_specs=placed, out_specs=P(SP_TP, None), check_vma=False
    )
```

profile of v0, /device:TPU:1, one launch (start us, length us, event | category | flops | bytes accessed | tf_op | source)
XLA Modules:
  0.0 285.0 jit_solution(6609689054624795851)
XLA Ops:
  6.5 1.3 fusion.67
  7.8 17.5 %psum.14 = f32[2,768]{1,0:T(2,128)S(1)} all-reduce(f32[2,768]{1,0:T(2,128)S(1)} %fusion.67), channel_id=1, replica_groups=mesh['sp_0'=8,'sp_1'=4,'tp'=8] {'sp_0'}, use_global_device_ids=true, to_apply=%region_0.1 | all-reduce | flops 1536 | bytes 12288 | tf_op jit(solution)/shard_map/psum | solution.py:17
  25.3 8.6 %psum.15 = f32[2,768]{1,0:T(2,128)S(1)} all-reduce(f32[2,768]{1,0:T(2,128)S(1)} %psum.14), channel_id=1, replica_groups=mesh['sp_0'=8,'sp_1'=4,'tp'=8] {'sp_1'}, use_global_device_ids=true, to_apply=%region_1.2 | all-reduce | flops 1536 | bytes 12288 | tf_op jit(solution)/shard_map/psum | solution.py:17
  33.9 19.5 %all_gather.15 = f32[2,6144]{1,0:T(2,128)S(1)} all-gather(f32[2,768]{1,0:T(2,128)S(1)} %psum.15), channel_id=1, replica_groups=mesh['sp_0'=8,'sp_1'=4,'tp'=8] {'tp'}, dimensions={1}, use_global_device_ids=true | all-gather | bytes 55296 | tf_op jit(solution)/shard_map/all_gather | solution.py:88
  53.4 1.1 fusion.28
  54.5 1.8 fusion.31
  56.5 23.1 %all-gather.4.cloned.1.call-done = bf16[512,2048]{1,0:T(8,128)(2,1)} async-done(((bf16[64,2048]{1,0:T(8,128)(2,1)}), bf16[512,2048]{1,0:T(8,128)(2,1)}) %all-gather.4.cloned.1.call-update) | async-done | bytes 2097168 | tf_op jit(solution)/shard_map/all_gather | solution.py:94
  79.5 2.5 multiply_reduce_fusion.3
  82.7 2.5 fusion.22
  86.8 3.0 %multiply_cosine_fusion.1 = (f32[512,32]{1,0:T(8,128)S(1)}, f32[512,32]{1,0:T(8,128)}, f32[512,32]{1,0:T(8,128)}, f32[512,32]{1,0:T(8,128)}) fusion(f32[32]{0:T(128)S(1)} %multiply_power_fusion, f32[512]{0:T(512)S(1)} %get-tuple-element.112, f32[512]{0:T(512)S(1)} %get-tuple-element.113), kind=kLoop, calls=%fused_computation.50 | loop fusion | flops 32768 | bytes 266368 | tf_op jit(solution)/shard_map/cos | solution.py:40
  89.9 1.3 fusion.23
  91.2 1.4 multiply_reduce_fusion.4
  92.6 40.4 %all_gather.17 = bf16[512,2,128]{2,0,1:T(8,128)(2,1)} all-gather(bf16[16,2,128]{2,0,1:T(8,128)(2,1)S(1)} %pad_maximum_fusion.2), channel_id=1, replica_groups=mesh['sp_0'=8,'sp_1'=4,'tp'=8] {'sp_0','sp_1'}, dimensions={0}, use_global_device_ids=true | all-gather | bytes 270336 | tf_op jit(solution)/shard_map/all_gather | solution.py:23
  133.1 1.6 multiply_reduce_fusion.2
  134.7 1.3 copy.16
  136.2 1.6 fusion.33
  139.6 46.4 %all-gather.6.cloned.1.call-done = bf16[16384,2,128]{0,2,1:T(8,128)(2,1)} async-done(((bf16[512,2,128]{0,2,1:T(8,128)(2,1)}), bf16[16384,2,128]{0,2,1:T(8,128)(2,1)}) %all-gather.6.cloned.1.call-update) | async-done | bytes 8388624 | tf_op jit(solution)/shard_map/all_gather | solution.py:23
  186.1 5.8 %fusion.76 = (bf16[16384,1,128]{0,2,1:T(8,128)(2,1)}, bf16[16384,1,128]{0,2,1:T(8,128)(2,1)}) fusion(bf16[16384,2,128]{0,2,1:T(8,128)(2,1)} %all-gather.6.cloned.1.call-done), kind=kLoop, calls=%fused_computation.126 | loop fusion | bytes 16777216 | tf_op jit(solution)/shard_map/slice | solution.py:25
  191.9 6.3 %copy.23 = bf16[16384,1,128]{2,0,1:T(8,128)(2,1)} copy(bf16[16384,1,128]{0,2,1:T(8,128)(2,1)} %get-tuple-element.78) | data formatting | bytes 8388608 | tf_op jit(solution)/shard_map/while | solution.py:172
  198.2 6.5 %copy.24 = bf16[16384,1,128]{2,0,1:T(8,128)(2,1)} copy(bf16[16384,1,128]{0,2,1:T(8,128)(2,1)} %get-tuple-element.77) | data formatting | bytes 8388608 | tf_op jit(solution)/shard_map/while | solution.py:172
  204.7 52.6 %while.14 = (s32[]{:T(128)}, f32[1,1024]{1,0:T(1,128)S(1)}, f32[1,1024]{1,0:T(1,128)S(1)}, f32[1,1024,128]{2,1,0:T(8,128)S(1)}, bf16[8,2048,1,128]{3,1,2,0:T(8,1...) while((s32[]{:T(128)}, f32[1,1024]{1,0:T(1,128)S(1)}, ...), condition=%wide.region_12.13_spmd, body=%wide.region_9.12_spmd.sunk | while | flops 1090783232 | bytes 27590756 | solution.py:172
  204.7 2.3 multiply_reduce_fusion.6
  207.0 1.4 fusion.96
  208.5 2.8 fusion.97
  211.3 2.3 multiply_reduce_fusion.6
  213.6 1.4 fusion.96
  215.1 2.8 fusion.97
  217.9 2.3 multiply_reduce_fusion.6
  220.2 1.4 fusion.96
  221.6 2.8 fusion.97
  224.4 2.3 multiply_reduce_fusion.6
  226.8 1.4 fusion.96
  228.2 2.8 fusion.97
  231.0 2.3 multiply_reduce_fusion.6
  233.3 1.4 fusion.96
  234.8 2.8 fusion.97
  237.6 2.3 multiply_reduce_fusion.6
  239.9 1.4 fusion.96
  241.4 2.8 fusion.97
  244.2 2.3 multiply_reduce_fusion.6
  246.5 1.4 fusion.96
  247.9 2.8 fusion.97
  250.7 2.3 multiply_reduce_fusion.6
  253.0 1.4 fusion.96
  254.5 2.8 fusion.97
  258.0 14.5 %all_to_all.19 = bf16[8,64,256]{2,1,0:T(8,128)(2,1)S(1)} all-to-all(bf16[8,64,256]{2,1,0:T(8,128)(2,1)S(1)} %all_to_all.14), channel_id=1, replica_groups=mesh['sp_0'=8,'sp_1'=4,'tp'=8] {'tp'}, dimensions={0} | all-to-all | bytes 524288 | tf_op jit(solution)/shard_map/all_to_all | solution.py:180
  272.5 5.1 %multiply_reduce_fusion.1 = (f32[64]{0:T(128)S(1)}, f32[64,2048]{1,0:T(8,128)S(1)}) fusion(bf16[64,2048]{1,0:T(8,128)(2,1)S(1)} %bitcast.110, bf16[2048,2048]{1,0:T(8,128)(2,1)} %all-gather.8.cloned.1.call-done), kind=kOutput, calls=%fused_computation.39 | convolution fusion | flops 537132992 | bytes 9175296 | tf_op jit(solution)/shard_map/dot_general | solution.py:181
  277.6 0.9 fusion.32
  (69 shorter events, 5.5 us)
Async XLA Ops:
  6.5 126.6 %copy-start = (bf16[2048,256]{1,0:T(8,128)(2,1)S(1)}, bf16[2048,256]{1,0:T(8,128)(2,1)}, u32[]{:S(2)}) copy-start(bf16[2048,256]{1,0:T(8,128)(2,1)} %param.18) | copy-start | bytes 3145732
  6.5 75.5 %copy-start.5 = (f32[128]{0:T(128)S(1)}, f32[128]{0:T(128)}, u32[]{:S(2)}) copy-start(f32[128]{0:T(128)} %param.23) | copy-start | bytes 1540
  6.5 73.0 %all-gather.4.cloned.1.call-start = ((), (), s32[]{:S(2)}) async-start(), calls=%async_computation.1 | async-start | bytes 2359296 | tf_op jit(solution)/shard_map/all_gather | solution.py:94
  56.4 129.7 %all-gather.6.cloned.1.call-start = ((), (), s32[]{:S(2)}) async-start(), calls=%async_computation.2 | async-start | bytes 8650752 | tf_op jit(solution)/shard_map/all_gather | solution.py:23
  56.4 33.3 %copy-start.4 = (bf16[16,2048]{1,0:T(8,128)(2,1)S(1)}, bf16[16,2048]{1,0:T(8,128)(2,1)}, u32[]{:S(2)}) copy-start(bf16[16,2048]{1,0:T(8,128)(2,1)} %param.14) | copy-start | bytes 196612
  82.1 51.0 %copy-start.1 = (bf16[512,2048]{1,0:T(8,128)(2,1)S(1)}, bf16[512,2048]{1,0:T(8,128)(2,1)}, u32[]{:S(2)}) copy-start(bf16[512,2048]{1,0:T(8,128)(2,1)} %all-gather.4.cloned.1.call-done) | copy-start | bytes 6291460
  86.0 49.9 %copy-start.6 = (f32[128]{0:T(128)S(1)}, f32[128]{0:T(128)}, u32[]{:S(2)}) copy-start(f32[128]{0:T(128)} %param.22) | copy-start | bytes 1540
  86.0 186.5 %all-gather.8.cloned.1.call-start = ((), (), s32[]{:S(2)}) async-start(), calls=%async_computation.3 | async-start | bytes 9437184 | tf_op jit(solution)/shard_map/all_gather | solution.py:183
  134.7 3.5 %copy-start.3 = (bf16[512,2,128]{2,0,1:T(8,128)(2,1)S(1)}, bf16[512,2,128]{2,0,1:T(8,128)(2,1)}, u32[]{:S(2)}) copy-start(bf16[512,2,128]{2,0,1:T(8,128)(2,1)} %all_gather.17) | copy-start | bytes 786436
  272.5 5.1 %copy-start.2 = (bf16[64,2048]{1,0:T(8,128)(2,1)S(1)}, bf16[64,2048]{1,0:T(8,128)(2,1)}, u32[]{:S(2)}) copy-start(bf16[64,2048]{1,0:T(8,128)(2,1)} %param.13) | copy-start | bytes 786436
Sparse Core Ops, SparseCore 0:
  56.5 23.0 all-gather.3
  86.1 99.8 all-gather.5
  187.9 54.6 all-gather.7
where the time goes:
time: 286 us; the launch traced here: 285 us
  blocking collectives  100 us (35%)
  waiting for transfers between devices  70.3 us (25%)
  matrix products  57.2 us (20%)
  other arithmetic  22.9 us (8%)
  local copies, waits for them, and re-layouts  20.4 us (7%)
  between operations  13.4 us (5%)
    all_gather x1, waiting for transfers between devices, side_by_side(): filled, at, done = (lax.all_gather(both, axis, axis=dim, tiled=True), 0, [])  46.4 us
    all_gather x1, blocking collectives, side_by_side(): filled, at, done = (lax.all_gather(both, axis, axis=dim, tiled=True), 0, [])  40.4 us
    psum x2, blocking collectives, over_axes(): value = lax.psum(value, axis)  26.1 us
    all_gather x1, waiting for transfers between devices, body(): piece = lax.all_gather(normalised_rows, 'tp', axis=0, tiled=True)  23.1 us
    dot_general x8, matrix products, update(): jnp.einsum('hqk,khd->hqd', weights_now.astype(jnp.bfloat16), value_block,...  22.2 us
    all_gather x1, blocking collectives, body(): modulation = lax.all_gather(summed, 'tp', axis=1, tiled=True)  19.5 us
    dot_general x8, matrix products, update(): jnp.einsum('hqd,khd->hqk', grouped, key_block, preferred_element_type=jnp...  18.4 us
    all_to_all x1, blocking collectives, body(): lax.all_to_all(attended, 'tp', split_axis=0, concat_axis=1, tiled=True)  14.5 us
  transfers between devices with their start and end apart: 3, of which 2 were waited for; matrix products, arithmetic and copies ran while one was open for 29% of the time, Pallas kernels for 0%

commit v1 on v0

--- a/solution.py
+++ b/solution.py
@@ -91,7 +91,9 @@
     prefix_normalised = modulate(context, modulation[1])
     query_cols = query_weight.shape[1]
     key_cols = key_matrix.shape[1]
-    piece = lax.all_gather(normalised_rows, "tp", axis=0, tiled=True)
+    piece = jnp.concatenate(
+        lax.all_to_all(jnp.stack([normalised_rows] * lax.axis_size("tp")), "tp", 0, 0), axis=0
+    )
     projected = jnp.concatenate(
         [
             jnp.dot(piece, query_weight, preferred_element_type=jnp.float32),

time: 286 us -> 285 us (level)
  waiting for transfers between devices: 70.3 us -> 80.3 us
  blocking collectives: 100 us -> 92.4 us
  other arithmetic: 22.9 us -> 17.8 us
  matrix products: 57.2 us -> 52.2 us
  starting transfers between devices: 0.09 us -> 4.1 us
    all_to_all x0 -> x1, waiting for transfers between devices: none -> 26.2 us  [body(): lax.all_to_all(jnp.stack([normalised_rows] * lax.axis_size('tp')), 'tp',...]
    all_gather x1 -> x0, waiting for transfers between devices: 23.1 us -> none  [body(): piece = lax.all_gather(normalised_rows, 'tp', axis=0, tiled=True)]
    all_gather x1, blocking collectives: 40.4 us -> 32.4 us  [side_by_side(): filled, at, done = (lax.all_gather(both, axis, axis=dim, tiled=True), 0, [])]
    all_gather x1, waiting for transfers between devices: 46.4 us -> 53.4 us  [side_by_side(): filled, at, done = (lax.all_gather(both, axis, axis=dim, tiled=True), 0, [])]
    all_to_all x0 -> x1, starting transfers between devices: none -> 4.06 us  [body(): lax.all_to_all(jnp.stack([normalised_rows] * lax.axis_size('tp')), 'tp',...]
  transfers between devices with their start and end apart: 3 -> 3, of which waited for: 2 -> 2; matrix products, arithmetic and copies ran while one was open for 29% -> 28% of each run, Pallas kernels for 0% -> 0%
where the time goes in v1:
time: 285 us; the launch traced here: 284 us
  blocking collectives  92.4 us (32%)
  waiting for transfers between devices  80.3 us (28%)
  matrix products  52.2 us (18%)
  local copies, waits for them, and re-layouts  23.2 us (8%)
  other arithmetic  17.8 us (6%)
  between operations  13.6 us (5%)
  starting transfers between devices  4.1 us (1%)
    all_gather x1, waiting for transfers between devices, side_by_side(): filled, at, done = (lax.all_gather(both, axis, axis=dim, tiled=True), 0, [])  53.4 us
    all_gather x1, blocking collectives, side_by_side(): filled, at, done = (lax.all_gather(both, axis, axis=dim, tiled=True), 0, [])  32.4 us
    all_to_all x1, waiting for transfers between devices, body(): lax.all_to_all(jnp.stack([normalised_rows] * lax.axis_size('tp')), 'tp',...  26.2 us
    psum x2, blocking collectives, over_axes(): value = lax.psum(value, axis)  26.1 us
    dot_general x8, matrix products, update(): jnp.einsum('hqk,khd->hqd', weights_now.astype(jnp.bfloat16), value_block,...  22.2 us
    all_gather x1, blocking collectives, body(): modulation = lax.all_gather(summed, 'tp', axis=1, tiled=True)  19.5 us
    dot_general x8, matrix products, update(): jnp.einsum('hqd,khd->hqk', grouped, key_block, preferred_element_type=jnp...  18.4 us
    all_to_all x1, blocking collectives, body(): lax.all_to_all(attended, 'tp', split_axis=0, concat_axis=1, tiled=True)  14.5 us
  transfers between devices with their start and end apart: 3, of which 2 were waited for; matrix products, arithmetic and copies ran while one was open for 28% of the time, Pallas kernels for 0%

profile of v1, /device:TPU:1, one launch (start us, length us, event | category | flops | bytes accessed | tf_op | source)
XLA Modules:
  0.0 284.0 jit_solution(8890586815705257067)
XLA Ops:
  6.5 1.3 fusion.67
  7.8 17.5 %psum.14 = f32[2,768]{1,0:T(2,128)S(1)} all-reduce(f32[2,768]{1,0:T(2,128)S(1)} %fusion.67), channel_id=1, replica_groups=mesh['sp_0'=8,'sp_1'=4,'tp'=8] {'sp_0'}, use_global_device_ids=true, to_apply=%region_0.1 | all-reduce | flops 1536 | bytes 12288 | tf_op jit(solution)/shard_map/psum | solution.py:17
  25.3 8.6 %psum.15 = f32[2,768]{1,0:T(2,128)S(1)} all-reduce(f32[2,768]{1,0:T(2,128)S(1)} %psum.14), channel_id=1, replica_groups=mesh['sp_0'=8,'sp_1'=4,'tp'=8] {'sp_1'}, use_global_device_ids=true, to_apply=%region_1.2 | all-reduce | flops 1536 | bytes 12288 | tf_op jit(solution)/shard_map/psum | solution.py:17
  33.9 19.5 %all_gather.12 = f32[2,6144]{1,0:T(2,128)S(1)} all-gather(f32[2,768]{1,0:T(2,128)S(1)} %psum.15), channel_id=1, replica_groups=mesh['sp_0'=8,'sp_1'=4,'tp'=8] {'tp'}, dimensions={1}, use_global_device_ids=true | all-gather | bytes 55296 | tf_op jit(solution)/shard_map/all_gather | solution.py:88
  53.4 1.1 fusion.28
  54.5 1.1 fusion.31
  55.6 1.6 stack.11
  57.2 4.1 %all-to-all-start = ((bf16[8,64,2048]{2,1,0:T(8,128)(2,1)}), bf16[8,64,2048]{2,1,0:T(8,128)(2,1)S(1)}, u32[]{:S(2)}, u32[]{:S(2)}) async-start(bf16[8,64,2048]{2,1,0:T(8,128)(2,1)} %stack.11), calls=%async_computation | async-start | bytes 4194304 | tf_op jit(solution)/shard_map/all_to_all | solution.py:95
  61.3 26.2 %all-to-all-done = bf16[8,64,2048]{2,1,0:T(8,128)(2,1)S(1)} async-done(((bf16[8,64,2048]{2,1,0:T(8,128)(2,1)}), bf16[8,64,2048]{2,1,0:T(8,128)(2,1)S(1)}, u32[]{:S(2)}, u32[]{:S(2)}) %all-to-all-start) | async-done | bytes 2097184 | tf_op jit(solution)/shard_map/all_to_all | solution.py:95
  87.5 0.8 fusion.22
  88.3 0.8 multiply_reduce_fusion.3
  89.9 0.7 pad_maximum_fusion
  90.7 0.7 all-gather.5.cloned.1.call-update
  92.7 2.3 copy.25
  95.1 32.4 %all_gather.13 = bf16[512,2,128]{2,0,1:T(8,128)(2,1)S(1)} all-gather(bf16[16,2,128]{2,0,1:T(8,128)(2,1)S(1)} %pad_maximum_fusion.1), channel_id=1, replica_groups=mesh['sp_0'=8,'sp_1'=4,'tp'=8] {'sp_0','sp_1'}, dimensions={0}, use_global_device_ids=true | all-gather | bytes 270336 | tf_op jit(solution)/shard_map/all_gather | solution.py:23
  127.4 2.0 multiply_reduce_fusion.2
  131.4 53.4 %all-gather.3.cloned.1.call-done = bf16[16384,2,128]{0,2,1:T(8,128)(2,1)} async-done(((bf16[512,2,128]{0,2,1:T(8,128)(2,1)}), bf16[16384,2,128]{0,2,1:T(8,128)(2,1)}) %all-gather.3.cloned.1.call-update) | async-done | bytes 8388624 | tf_op jit(solution)/shard_map/all_gather | solution.py:23
  184.7 5.8 %fusion.76 = (bf16[16384,1,128]{0,2,1:T(8,128)(2,1)}, bf16[16384,1,128]{0,2,1:T(8,128)(2,1)}) fusion(bf16[16384,2,128]{0,2,1:T(8,128)(2,1)} %all-gather.3.cloned.1.call-done), kind=kLoop, calls=%fused_computation.126 | loop fusion | bytes 16777216 | tf_op jit(solution)/shard_map/slice | solution.py:25
  190.5 6.3 %copy.26 = bf16[16384,1,128]{2,0,1:T(8,128)(2,1)} copy(bf16[16384,1,128]{0,2,1:T(8,128)(2,1)} %get-tuple-element.78) | data formatting | bytes 8388608 | tf_op jit(solution)/shard_map/while | solution.py:174
  196.9 6.5 %copy.27 = bf16[16384,1,128]{2,0,1:T(8,128)(2,1)} copy(bf16[16384,1,128]{0,2,1:T(8,128)(2,1)} %get-tuple-element.77) | data formatting | bytes 8388608 | tf_op jit(solution)/shard_map/while | solution.py:174
  203.4 52.6 %while.14 = (s32[]{:T(128)}, f32[1,1024]{1,0:T(1,128)S(1)}, f32[1,1024]{1,0:T(1,128)S(1)}, f32[1,1024,128]{2,1,0:T(8,128)S(1)}, bf16[8,2048,1,128]{3,1,2,0:T(8,1...) while((s32[]{:T(128)}, f32[1,1024]{1,0:T(1,128)S(1)}, ...), condition=%wide.region_12.13_spmd, body=%wide.region_9.12_spmd.sunk | while | flops 1090783232 | bytes 27590756 | solution.py:174
  203.4 2.3 multiply_reduce_fusion.6
  205.7 1.4 fusion.96
  207.2 2.8 fusion.97
  210.0 2.3 multiply_reduce_fusion.6
  212.3 1.4 fusion.96
  213.7 2.8 fusion.97
  216.5 2.3 multiply_reduce_fusion.6
  218.8 1.4 fusion.96
  220.3 2.8 fusion.97
  223.1 2.3 multiply_reduce_fusion.6
  225.4 1.4 fusion.96
  226.9 2.8 fusion.97
  229.7 2.3 multiply_reduce_fusion.6
  232.0 1.4 fusion.96
  233.5 2.8 fusion.97
  236.3 2.3 multiply_reduce_fusion.6
  238.6 1.4 fusion.96
  240.0 2.8 fusion.97
  242.8 2.3 multiply_reduce_fusion.6
  245.1 1.4 fusion.96
  246.6 2.8 fusion.97
  249.4 2.3 multiply_reduce_fusion.6
  251.7 1.4 fusion.96
  253.2 2.8 fusion.97
  256.6 14.5 %all_to_all.24 = bf16[8,64,256]{2,1,0:T(8,128)(2,1)S(1)} all-to-all(bf16[8,64,256]{2,1,0:T(8,128)(2,1)S(1)} %all_to_all.18), channel_id=1, replica_groups=mesh['sp_0'=8,'sp_1'=4,'tp'=8] {'tp'}, dimensions={0} | all-to-all | bytes 524288 | tf_op jit(solution)/shard_map/all_to_all | solution.py:182
  271.2 5.1 %multiply_reduce_fusion.1 = (f32[64]{0:T(128)S(1)}, f32[64,2048]{1,0:T(8,128)S(1)}) fusion(bf16[64,2048]{1,0:T(8,128)(2,1)S(1)} %bitcast.115, bf16[2048,2048]{1,0:T(8,128)(2,1)} %all-gather.5.cloned.1.call-done), kind=kOutput, calls=%fused_computation.39 | convolution fusion | flops 537132992 | bytes 9175296 | tf_op jit(solution)/shard_map/dot_general | solution.py:183
  276.3 0.9 fusion.32
  (68 shorter events, 5.0 us)
Async XLA Ops:
  6.5 81.8 %copy-start = (bf16[2048,128]{1,0:T(8,128)(2,1)S(1)}, bf16[2048,128]{1,0:T(8,128)(2,1)}, u32[]{:S(2)}) copy-start(bf16[2048,128]{1,0:T(8,128)(2,1)} %param.19) | copy-start | bytes 1572868
  6.5 81.0 %copy-start.2 = (bf16[2048,128]{1,0:T(8,128)(2,1)S(1)}, bf16[2048,128]{1,0:T(8,128)(2,1)}, u32[]{:S(2)}) copy-start(bf16[2048,128]{1,0:T(8,128)(2,1)} %param.20) | copy-start | bytes 1572868
  57.2 32.0 %copy-start.4 = (f32[128]{0:T(128)S(1)}, f32[128]{0:T(128)}, u32[]{:S(2)}) copy-start(f32[128]{0:T(128)} %param.23) | copy-start | bytes 1540
  57.2 30.3 %all-to-all-start = ((bf16[8,64,2048]{2,1,0:T(8,128)(2,1)}), bf16[8,64,2048]{2,1,0:T(8,128)(2,1)S(1)}, u32[]{:S(2)}, u32[]{:S(2)}) async-start(bf16[8,64,2048]{2,1,0:T(8,128)(2,1)} %stack.11), calls=%async_computation | async-start | bytes 4194304 | tf_op jit(solution)/shard_map/all_to_all | solution.py:95
  61.3 123.4 %all-gather.3.cloned.1.call-start = ((), (), s32[]{:S(2)}) async-start(), calls=%async_computation.2 | async-start | bytes 8650752 | tf_op jit(solution)/shard_map/all_gather | solution.py:23
  87.5 4.4 %copy-start.3 = (bf16[16,2048]{1,0:T(8,128)(2,1)S(1)}, bf16[16,2048]{1,0:T(8,128)(2,1)}, u32[]{:S(2)}) copy-start(bf16[16,2048]{1,0:T(8,128)(2,1)} %param.14) | copy-start | bytes 196612
  90.6 180.5 %all-gather.5.cloned.1.call-start = ((), (), s32[]{:S(2)}) async-start(), calls=%async_computation.3 | async-start | bytes 9437184 | tf_op jit(solution)/shard_map/all_gather | solution.py:185
  91.9 37.5 %copy-start.5 = (f32[128]{0:T(128)S(1)}, f32[128]{0:T(128)}, u32[]{:S(2)}) copy-start(f32[128]{0:T(128)} %param.22) | copy-start | bytes 1540
  271.2 5.1 %copy-start.1 = (bf16[64,2048]{1,0:T(8,128)(2,1)S(1)}, bf16[64,2048]{1,0:T(8,128)(2,1)}, u32[]{:S(2)}) copy-start(bf16[64,2048]{1,0:T(8,128)(2,1)} %param.13) | copy-start | bytes 786436
Sparse Core Ops, SparseCore 0:
  90.7 93.9 all-gather.2
  186.6 54.6 all-gather.4
